TPU v7x, 32 devices: a whole 2x2x4 slice. The times are simulated.
32 devices in a mesh: dp: 4 (over y, x), kv: 4 (over z), tp: 2 (over core).
Axes of the slice: x: 2, y: 2, z: 4, core: 2. Of those that a mesh axis runs over, the one named last changes fastest.
Arguments:
- tokens: bfloat16 [4, 16, 2048], P('dp', None, 'kv'), may hold values from -18 to 18, as said below
- norm_gain: float32 [2048], P('kv'), may hold values from 0.1 to 1.9
- w_query: bfloat16 [2048, 3072], P('kv', 'tp'), may hold values from -0.125 to 0.125
- w_key: bfloat16 [2048, 3072], P('kv', 'tp'), may hold values from -0.125 to 0.125
- w_value: bfloat16 [2048, 3072], P('kv', 'tp'), may hold values from -0.125 to 0.125
- w_gate: bfloat16 [2048, 3072], P('kv', 'tp'), may hold values from -0.125 to 0.125
- w_out: bfloat16 [3072, 2048], P('tp', 'kv'), may hold values from -0.109375 to 0.109375
- head_bias: float32 [24], P('tp'), may hold values from -14 to -2
- cache_keys: bfloat16 [4, 2048, 24, 128], P('dp', 'kv', 'tp'), may hold values from -18 to 18, as said below
- cache_values: bfloat16 [4, 2048, 24, 128], P('dp', 'kv', 'tp'), may hold values from -6 to 6
- prefix_len: int32 [4], P('dp'), may hold values from 1536 to 2028
- accepted: int32 [4], P('dp'), may hold values from 1 to 4
- parent: int32 [4, 16], P('dp'), may hold values from -1 to 14, as said below
Outputs:
- mixed: bfloat16 [4, 16, 2048], P('dp', None, 'kv')
- keys_next: bfloat16 [4, 2048, 24, 128], P('dp', 'kv', 'tp')
- values_next: bfloat16 [4, 2048, 24, 128], P('dp', 'kv', 'tp')
Inputs may be any that keep to these rules, and one draw needn't show every extreme that they name: `tokens`: entries of order one. `cache_keys`: entries of order one. parent of proposal 0 is -1; for p of 1 or more, parent[p] lies in max(p - 3, 0) to p - 1.
All inputs are finite; a program needn't handle non-finite values.
Results may differ from a plain program's by a relative error of at most 0.012.
Values may be sent and summed in bfloat16 or wider, within the bound.
A program may use at most 64 MiB of HBM per device.

v0:
```python
import jax
import jax.numpy as jnp
from jax import lax
from jax.sharding import PartitionSpec as P

D = 2048
HEAD = 128
EPS = 1e-06


def ancestry(parent):
    count = parent.shape[-1]
    places = jnp.arange(count, dtype=jnp.int32)
    reach = (parent[:, :, None] == places[None, None, :]).astype(jnp.float32)
    for repeat in range(count.bit_length()):
        reach = jnp.minimum(
            reach + jnp.einsum("spj,sjk->spk", reach, reach, precision=lax.Precision.HIGHEST), 1.0
        )
    return reach > 0.5


def after_table(count):
    places = jnp.arange(count, dtype=jnp.int32)
    return (places[:, None] > places[None, :]).astype(jnp.float32)


def sum_after(values):
    table = after_table(values.shape[-1])
    return jnp.einsum("shpk,kc->shpc", values, table, precision=lax.Precision.HIGHEST)


def local(
    tokens,
    norm_gain,
    w_query,
    w_key,
    w_value,
    w_gate,
    w_out,
    head_bias,
    cache_keys,
    cache_values,
    prefix_len,
    accepted,
    parent,
):
    seqs, props, columns = tokens.shape
    width = w_query.shape[1]
    heads = width // HEAD
    flat = tokens.astype(jnp.float32).reshape(seqs * props, columns)
    square_part = jnp.sum(flat * flat, axis=1)
    scaled = (flat * norm_gain).astype(jnp.bfloat16)
    partial_value = jnp.concatenate(
        [
            jnp.dot(scaled, weight, preferred_element_type=jnp.float32)
            for weight in (w_query, w_key, w_value, w_gate)
        ],
        axis=1,
    )
    squares = lax.psum(square_part, "kv")
    share = lax.psum_scatter(partial_value, "kv", scatter_dimension=1, tiled=True)
    rscale = lax.rsqrt(squares / D + EPS)
    projected = lax.all_gather(
        (share * rscale[:, None]).astype(jnp.bfloat16), "kv", axis=1, tiled=True
    )
    shaped = projected.reshape(seqs, props, 4, heads, HEAD)
    query = shaped[:, :, 0]
    key_new = shaped[:, :, 1]
    value_new = shaped[:, :, 2]
    gate = projected[:, 3 * width :].astype(jnp.float32)
    factor = HEAD ** (-0.5)
    bias_col = head_bias[None, :, None, None]
    ctx_dev = cache_keys.shape[1]
    places = lax.axis_index("kv") * ctx_dev + jnp.arange(ctx_dev, dtype=jnp.int32)
    valid = prefix_len + accepted
    live = (places[None, :] < valid[:, None])[:, None, None, :]
    scores = (
        jnp.einsum("sphd,schd->shpc", query, cache_keys, preferred_element_type=jnp.float32)
        * factor
        + bias_col
    )
    keep_log = jnp.where(live, jax.nn.log_sigmoid(-scores), 0.0)
    shard_rest = jnp.sum(keep_log, axis=3)
    family = ancestry(parent)[:, None]
    tree_scores = (
        jnp.einsum("sphd,sjhd->shpj", query, key_new, preferred_element_type=jnp.float32) * factor
        + bias_col
    )
    tree_keep = jnp.where(family, jax.nn.log_sigmoid(-tree_scores), 0.0)
    tail = jnp.sum(tree_keep, axis=3)
    every = lax.all_gather(shard_rest[None], "kv", axis=0, tiled=True)
    after = jnp.arange(every.shape[0], dtype=jnp.int32) > lax.axis_index("kv")
    beyond = jnp.sum(jnp.where(after[:, None, None, None], every, 0.0), axis=0)
    later_cache = sum_after(keep_log) + (beyond + tail)[..., None]
    cache_weight = jnp.where(live, jnp.exp(jax.nn.log_sigmoid(scores) + later_cache), 0.0).astype(
        jnp.bfloat16
    )
    later_tree = sum_after(tree_keep)
    tree_weight = jnp.where(
        family, jnp.exp(jax.nn.log_sigmoid(tree_scores) + later_tree), 0.0
    ).astype(jnp.bfloat16)
    local_sum = jnp.einsum(
        "shpc,schd->sphd", cache_weight, cache_values, preferred_element_type=jnp.float32
    )
    attended = lax.psum(local_sum, "kv")
    attended = attended + jnp.einsum(
        "shpj,sjhd->sphd", tree_weight, value_new, preferred_element_type=jnp.float32
    )
    mixin = (attended.reshape(seqs * props, width) * jax.nn.silu(gate)).astype(jnp.bfloat16)
    part_out = jnp.dot(mixin, w_out, preferred_element_type=jnp.float32).astype(jnp.bfloat16)
    part_out = lax.optimization_barrier(part_out).astype(jnp.float32)
    mixed = lax.psum(part_out.astype(jnp.bfloat16), "tp").reshape(seqs, props, w_out.shape[1])
    relative = places[None, :] - valid[:, None]
    picker = (relative[:, :, None] == jnp.arange(props, dtype=jnp.int32)[None, None, :]).astype(
        jnp.bfloat16
    )
    inside = ((relative >= 0) & (relative < props))[:, :, None, None]
    placed_keys = jnp.einsum(
        "scp,sphd->schd", picker, key_new, preferred_element_type=jnp.float32
    ).astype(jnp.bfloat16)
    placed_values = jnp.einsum(
        "scp,sphd->schd", picker, value_new, preferred_element_type=jnp.float32
    ).astype(jnp.bfloat16)
    keys_next = jnp.where(inside, placed_keys, cache_keys)
    values_next = jnp.where(inside, placed_values, cache_values)
    return (mixed, keys_next, values_next)


def solution(mesh):
    return jax.shard_map(
        local,
        mesh=mesh,
        in_specs=(
            P("dp", None, "kv"),
            P("kv"),
            P("kv", "tp"),
            P("kv", "tp"),
            P("kv", "tp"),
            P("kv", "tp"),
            P("tp", "kv"),
            P("tp"),
            P("dp", "kv", "tp", None),
            P("dp", "kv", "tp", None),
            P("dp"),
            P("dp"),
            P("dp", None),
        ),
        out_specs=(P("dp", None, "kv"), P("dp", "kv", "tp", None), P("dp", "kv", "tp", None)),
        check_vma=False,
    )
```

profile of v0, /device:TPU:0, one launch (start us, length us, event | category | flops | bytes accessed | tf_op | source)
XLA Modules:
  0.0 114.4 jit_solution(16729290940814623827)
XLA Ops:
  7.2 0.0 copy-start
  7.2 0.0 copy-start.8
  7.2 0.0 copy-start.11
  7.2 0.0 copy-start.4
  7.2 0.0 reduce-scatter.2.cloned.1.call-start
  7.3 1.3 %copy-done = bf16[512,1536]{1,0:T(8,128)(2,1)S(1)} copy-done((bf16[512,1536]{1,0:T(8,128)(2,1)S(1)}, bf16[512,1536]{1,0:T(8,128)(2,1)}, u32[]{:S(2)}) %copy-start) | copy-done | bytes 1572888
  8.6 0.0 copy-start.5
  8.6 1.1 fusion.70
  9.7 0.0 copy-done.8
  9.7 0.0 copy-done.11
  9.7 0.0 copy-done.4
  9.8 0.0 copy-start.6
  9.8 0.3 fusion.68
  10.1 0.1 copy-done.5
  10.1 0.3 fusion.66
  10.4 0.8 copy-done.6
  11.3 0.0 copy-start.13
  11.3 0.3 fusion.64
  11.6 0.0 copy-start.12
  11.6 0.0 copy-start.1
  11.6 0.8 pad_maximum_fusion
  12.4 0.0 reduce-scatter.2.cloned.1.call-update
  12.4 0.0 all-reduce.2.cloned.1.call-start
  12.4 0.0 copy-done.13
  12.4 0.2 fusion.26
  12.6 0.1 fusion.22
  12.8 0.1 fusion.23
  12.9 0.1 fusion.24
  13.0 0.2 fusion.27
  14.5 0.1 copy.29
  14.6 0.1 fusion.52
  14.7 13.6 %psum.21 = f32[16]{0:T(128)S(1)} all-reduce(f32[16]{0:T(128)S(1)} %fusion.52), channel_id=1, replica_groups=mesh['dp'=4,'kv'=4,'tp'=2] {'kv'}, use_global_device_ids=true, to_apply=%region_2.0 | all-reduce | flops 16 | bytes 128 | tf_op jit(solution)/shard_map/psum | solution.py:60
  28.4 7.6 %reduce-scatter.2.cloned.1.call-done = f32[16,1536]{1,0:T(8,128)} async-done(((f32[16,6144]{1,0:T(8,128)}), f32[16,1536]{1,0:T(8,128)}) %reduce-scatter.2.cloned.1.call-update) | async-done | bytes 98320 | tf_op jit(solution)/shard_map/reduce_scatter | solution.py:61
  36.0 1.0 multiply_convert_fusion
  37.0 13.6 %all_gather.6 = bf16[16,6144]{1,0:T(8,128)(2,1)S(1)} all-gather(bf16[16,1536]{1,0:T(8,128)(2,1)S(1)} %multiply_convert_fusion), channel_id=1, replica_groups=mesh['dp'=4,'kv'=4,'tp'=2] {'kv'}, dimensions={1}, use_global_device_ids=true | all-gather | bytes 245760 | tf_op jit(solution)/shard_map/all_gather | solution.py:63
  50.6 0.9 reshape.356
  51.4 0.9 fusion.80
  52.4 0.0 copy-done.12
  52.4 0.2 fusion.45
  52.5 0.0 copy-done.1
  52.5 0.0 copy-start.9
  52.6 0.5 fusion.32
  53.1 0.3 fusion.31
  53.4 13.2 %all-gather.1 = f32[4,12,16]{2,1,0:T(8,128)S(1)} all-gather(f32[1,12,16]{2,1,0:T(8,128)S(1)} %bitcast.103), channel_id=2, replica_groups=mesh['dp'=4,'kv'=4,'tp'=2] {'kv'}, dimensions={0}, use_global_device_ids=true | all-gather | bytes 3840 | tf_op jit(solution)/shard_map/all_gather | solution.py:91
  66.6 0.1 fusion.53
  66.6 0.1 fusion.43
  66.7 0.0 copy-start.2
  66.8 0.9 fusion.13
  67.7 0.0 copy-done.9
  67.7 0.5 copy-done.2
  68.2 1.0 fusion.14
  69.1 0.0 all-reduce.2.cloned.1.call-update
  69.1 0.0 copy-start.3
  69.2 1.8 %bitcast_select_fusion.1 = bf16[1,512,12,128]{3,1,2,0:T(8,128)(2,1)} fusion(bf16[1,512,12,128]{3,1,2,0:T(8,128)(2,1)S(1)} %copy-done.1, pred[512]{0:T(512)(128)(4,1)S(1)} %compare_and_fusion, bf16[1,16,1,12,128]{4,3,2,1,0:T(8,128)(2,1)S(1)} %get-tuple-element.4, s32[512]{0:T(512)S(1)} %fusion.73), kind=kOutput, calls=%fused_computation.3 | convolution fusion | flops 26746880 | bytes 3197440 | tf_op jit(solution)/shard_map/scp,sphd->schd/dot_general | solution.py:118
  70.9 0.0 copy-done.3
  70.9 0.0 copy-start.10
  70.9 1.8 %bitcast_select_fusion = bf16[1,512,12,128]{3,1,2,0:T(8,128)(2,1)} fusion(bf16[1,512,12,128]{3,1,2,0:T(8,128)(2,1)S(1)} %copy-done.3, pred[512]{0:T(512)(128)(4,1)S(1)} %compare_and_fusion, bf16[1,16,1,12,128]{4,3,2,1,0:T(8,128)(2,1)S(1)} %get-tuple-element.3, s32[512]{0:T(512)S(1)} %fusion.73), kind=kOutput, calls=%fused_computation.2 | convolution fusion | flops 26746880 | bytes 3197440 | tf_op jit(solution)/shard_map/scp,sphd->schd/dot_general | solution.py:121
  72.7 0.0 copy-done.10
  72.7 0.3 fusion.21
  73.0 29.2 %all-reduce.2.cloned.1.call-done = f32[1,16,12,128]{3,1,2,0:T(8,128)} async-done(((f32[1,16,12,128]{3,1,2,0:T(8,128)}), f32[1,16,12,128]{3,1,2,0:T(8,128)}) %all-reduce.2.cloned.1.call-update) | async-done | bytes 98320 | tf_op jit(solution)/shard_map/psum | solution.py:105
  102.2 1.1 fusion.17
  103.3 0.0 copy-done.7
  103.3 0.3 convolution_convert_fusion.2
  103.6 4.0 %psum.23 = bf16[1,16,512]{2,1,0:T(8,128)(2,1)} all-reduce(bf16[1,16,512]{2,1,0:T(8,128)(2,1)S(1)} %bitcast.102), channel_id=1, replica_groups=mesh['dp'=4,'kv'=4,'tp'=2] {'tp'}, use_global_device_ids=true, to_apply=%region_7.8 | all-reduce | flops 8192 | bytes 32768 | tf_op jit(solution)/shard_map/psum | solution.py:112
  (8 shorter events, 0.1 us)
Async XLA Ops:
  7.2 1.4 %copy-start = (bf16[512,1536]{1,0:T(8,128)(2,1)S(1)}, bf16[512,1536]{1,0:T(8,128)(2,1)}, u32[]{:S(2)}) copy-start(bf16[512,1536]{1,0:T(8,128)(2,1)} %param.15) | copy-start | bytes 4718596
  7.2 2.5 %copy-start.8 = (bf16[1,16,512]{2,1,0:T(8,128)(2,1)S(1)}, bf16[1,16,512]{2,1,0:T(8,128)(2,1)}, u32[]{:S(2)}) copy-start(bf16[1,16,512]{2,1,0:T(8,128)(2,1)} %param.13) | copy-start | bytes 49156
  7.2 2.5 %copy-start.11 = (f32[512]{0:T(512)S(1)}, f32[512]{0:T(512)}, u32[]{:S(2)}) copy-start(f32[512]{0:T(512)} %param.14) | copy-start | bytes 6148
  7.2 2.5 %copy-start.4 = (bf16[512,1536]{1,0:T(8,128)(2,1)S(1)}, bf16[512,1536]{1,0:T(8,128)(2,1)}, u32[]{:S(2)}) copy-start(bf16[512,1536]{1,0:T(8,128)(2,1)} %param.16) | copy-start | bytes 4718596
  7.2 28.8 %reduce-scatter.2.cloned.1.call-start = ((), (), s32[]{:S(2)}) async-start(), calls=%async_computation.1 | async-start | bytes 491520 | tf_op jit(solution)/shard_map/reduce_scatter | solution.py:61
  8.6 1.6 %copy-start.5 = (bf16[512,1536]{1,0:T(8,128)(2,1)S(1)}, bf16[512,1536]{1,0:T(8,128)(2,1)}, u32[]{:S(2)}) copy-start(bf16[512,1536]{1,0:T(8,128)(2,1)} %param.17) | copy-start | bytes 4718596
  9.8 1.5 %copy-start.6 = (bf16[512,1536]{1,0:T(8,128)(2,1)S(1)}, bf16[512,1536]{1,0:T(8,128)(2,1)}, u32[]{:S(2)}) copy-start(bf16[512,1536]{1,0:T(8,128)(2,1)} %param.18) | copy-start | bytes 4718596
  11.3 1.2 %copy-start.13 = (s32[1,16]{1,0:T(1,128)S(1)}, s32[1,16]{1,0:T(1,128)}, u32[]{:S(2)}) copy-start(s32[1,16]{1,0:T(1,128)} %param.25) | copy-start | bytes 196
  11.6 40.8 %copy-start.12 = (f32[12]{0:T(128)S(1)}, f32[12]{0:T(128)}, u32[]{:S(2)}) copy-start(f32[12]{0:T(128)} %param.20) | copy-start | bytes 148
  11.6 41.0 %copy-start.1 = (bf16[1,512,12,128]{3,1,2,0:T(8,128)(2,1)S(1)}, bf16[1,512,12,128]{3,1,2,0:T(8,128)(2,1)}, u32[]{:S(2)}) copy-start(bf16[1,512,12,128]{3,1,2,0:T(8,128)(2,1)} %param.21) | copy-start | bytes 4718596
  12.4 89.8 %all-reduce.2.cloned.1.call-start = ((), (), s32[]{:S(2)}) async-start(), calls=%async_computation.2 | async-start | bytes 196608 | tf_op jit(solution)/shard_map/psum | solution.py:105
  52.5 15.1 %copy-start.9 = (f32[12,16,16]{1,2,0:T(8,128)}, f32[12,16,16]{1,2,0:T(8,128)S(1)}, u32[]{:S(2)}) copy-start(f32[12,16,16]{1,2,0:T(8,128)S(1)} %get-tuple-element.9) | copy-start | bytes 36868
  66.7 1.4 %copy-start.2 = (bf16[1,512,12,128]{3,1,2,0:T(8,128)(2,1)S(1)}, bf16[1,512,12,128]{3,1,2,0:T(8,128)(2,1)}, u32[]{:S(2)}) copy-start(bf16[1,512,12,128]{3,1,2,0:T(8,128)(2,1)} %param.22) | copy-start | bytes 4718596
  69.1 1.8 %copy-start.3 = (bf16[1,512,12,128]{3,1,2,0:T(8,128)(2,1)S(1)}, bf16[1,512,12,128]{3,1,2,0:T(8,128)(2,1)}, u32[]{:S(2)}) copy-start(bf16[1,512,12,128]{3,1,2,0:T(8,128)(2,1)} %param.22) | copy-start | bytes 4718596
  70.9 1.8 %copy-start.10 = (f32[12,16,16]{1,2,0:T(8,128)S(1)}, f32[12,16,16]{1,2,0:T(8,128)}, u32[]{:S(2)}) copy-start(f32[12,16,16]{1,2,0:T(8,128)} %copy-done.9) | copy-start | bytes 36868
  70.9 32.4 %copy-start.7 = (bf16[1536,512]{1,0:T(8,128)(2,1)S(1)}, bf16[1536,512]{1,0:T(8,128)(2,1)}, u32[]{:S(2)}) copy-start(bf16[1536,512]{1,0:T(8,128)(2,1)} %param.19) | copy-start | bytes 4718596
Sparse Core Ops, SparseCore 0:
  12.5 23.4 reduce-scatter.1
  69.3 32.8 all-reduce.1
where the time goes:
time: 115 us; the launch traced here: 114 us
  blocking collectives  44.4 us (39%)
  waiting for transfers between devices  36.8 us (32%)
  between operations  15.6 us (14%)
  matrix products  10.6 us (9%)
  local copies, waits for them, and re-layouts  4.63 us (4%)
  other arithmetic  2.38 us (2%)
    psum x1, waiting for transfers between devices, local(): attended = lax.psum(local_sum, 'kv')  29.2 us
    psum x1, blocking collectives, local(): squares = lax.psum(square_part, 'kv')  13.6 us
    all_gather x1, blocking collectives, local(): lax.all_gather((share * rscale[:, None]).astype(jnp.bfloat16), 'kv', axis...  13.6 us
    all_gather x1, blocking collectives, local(): every = lax.all_gather(shard_rest[None], 'kv', axis=0, tiled=True)  13.2 us
    reduce_scatter x1, waiting for transfers between devices, local(): lax.psum_scatter(partial_value, 'kv', scatter_dimension=1, tiled=True)  7.6 us
    psum x1, blocking collectives, local(): lax.psum(part_out.astype(jnp.bfloat16), 'tp')  3.96 us
    unnamed x28, local copies, waits for them, and re-layouts  2.74 us
  transfers between devices with their start and end apart: 2, of which 2 were waited for; matrix products, arithmetic and copies ran while one was open for 4% of the time, Pallas kernels for 0%

commit v1 on v0

--- a/solution.py
+++ b/solution.py
@@ -102,7 +102,8 @@
     local_sum = jnp.einsum(
         "shpc,schd->sphd", cache_weight, cache_values, preferred_element_type=jnp.float32
     )
-    attended = lax.psum(local_sum, "kv")
+    seen_now = lax.all_gather(local_sum, axis_name="kv")
+    attended = jnp.sum(seen_now, axis=0)
     attended = attended + jnp.einsum(
         "shpj,sjhd->sphd", tree_weight, value_new, preferred_element_type=jnp.float32
     )

time: 115 us -> 101 us (0.88)
  waiting for transfers between devices: 36.8 us -> 7.76 us
  blocking collectives: 44.4 us -> 58.6 us
    psum x1 -> x0, waiting for transfers between devices: 29.2 us -> none  [local(): attended = lax.psum(local_sum, 'kv')]
    all_gather x0 -> x1, blocking collectives: none -> 14.2 us  [local(): seen_now = lax.all_gather(local_sum, axis_name='kv')]
    unnamed x28 -> x26, local copies, waits for them, and re-layouts: 2.74 us -> 2.74 us
  transfers between devices with their start and end apart: 2 -> 1, of which waited for: 2 -> 1; matrix products, arithmetic and copies ran while one was open for 4% -> 1% of each run, Pallas kernels for 0% -> 0%
where the time goes in v1:
time: 101 us
  blocking collectives  58.6 us (58%)
  between operations  15.5 us (15%)
  matrix products  11.4 us (11%)
  waiting for transfers between devices  7.76 us (8%)
  local copies, waits for them, and re-layouts  4.63 us (5%)
  other arithmetic  3.04 us (3%)
    all_gather x1, blocking collectives, local(): seen_now = lax.all_gather(local_sum, axis_name='kv')  14.2 us
    all_gather x1, blocking collectives, local(): lax.all_gather((share * rscale[:, None]).astype(jnp.bfloat16), 'kv', axis...  13.6 us
    psum x1, blocking collectives, local(): squares = lax.psum(square_part, 'kv')  13.6 us
    all_gather x1, blocking collectives, local(): every = lax.all_gather(shard_rest[None], 'kv', axis=0, tiled=True)  13.2 us
    reduce_scatter x1, waiting for transfers between devices, local(): lax.psum_scatter(partial_value, 'kv', scatter_dimension=1, tiled=True)  7.74 us
    psum x1, blocking collectives, local(): lax.psum(part_out.astype(jnp.bfloat16), 'tp')  3.96 us
    unnamed x26, local copies, waits for them, and re-layouts  2.74 us
    dot_general x4, matrix products, local(): jnp.dot(scaled, weight, preferred_element_type=jnp.float32)  2.06 us
  transfers between devices with their start and end apart: 1, of which 1 were waited for; matrix products, arithmetic and copies ran while one was open for 1% of the time, Pallas kernels for 0%

profile of v1, /device:TPU:0, one launch (start us, length us, event | category | flops | bytes accessed | tf_op | source)
XLA Modules:
  0.0 101.0 jit_solution(7498128047702497777)
XLA Ops:
  7.2 0.0 copy-start
  7.2 0.0 copy-start.8
  7.2 0.0 copy-start.10
  7.2 0.0 copy-start.3
  7.2 0.0 reduce-scatter.2.cloned.1.call-start
  7.3 1.3 %copy-done = bf16[512,1536]{1,0:T(8,128)(2,1)S(1)} copy-done((bf16[512,1536]{1,0:T(8,128)(2,1)S(1)}, bf16[512,1536]{1,0:T(8,128)(2,1)}, u32[]{:S(2)}) %copy-start) | copy-done | bytes 1572888
  8.6 0.0 copy-start.4
  8.6 1.1 %fusion.70 = f32[16,1536]{1,0:T(8,128)S(1)} fusion(bf16[512,1536]{1,0:T(8,128)(2,1)S(1)} %copy-done, bf16[1,16,512]{2,1,0:T(8,128)(2,1)} %param.13, f32[512]{0:T(512)} %param.14), kind=kOutput, calls=%fused_computation.92 | convolution fusion | flops 25190400 | bytes 1689600 | tf_op jit(solution)/shard_map/dot_general | solution.py:55
  9.7 0.0 copy-done.8
  9.7 0.0 copy-done.10
  9.7 0.0 copy-done.3
  9.8 0.0 copy-start.5
  9.8 0.3 fusion.68
  10.1 0.1 copy-done.4
  10.1 0.3 fusion.66
  10.4 0.8 copy-done.5
  11.3 0.0 copy-start.12
  11.3 0.3 fusion.64
  11.6 0.0 copy-start.11
  11.6 0.8 pad_maximum_fusion
  12.4 0.0 copy-start.1
  12.4 0.0 reduce-scatter.2.cloned.1.call-update
  12.4 0.0 copy-done.12
  12.4 0.2 fusion.26
  12.6 0.1 fusion.22
  12.7 0.1 fusion.23
  12.9 0.1 fusion.24
  13.0 0.2 fusion.27
  14.5 0.1 copy.29
  14.5 0.1 fusion.52
  14.7 13.6 %psum.14 = f32[16]{0:T(128)S(1)} all-reduce(f32[16]{0:T(128)S(1)} %fusion.52), channel_id=1, replica_groups=mesh['dp'=4,'kv'=4,'tp'=2] {'kv'}, use_global_device_ids=true, to_apply=%region_2.0 | all-reduce | flops 16 | bytes 128 | tf_op jit(solution)/shard_map/psum | solution.py:60
  28.3 7.7 %reduce-scatter.2.cloned.1.call-done = f32[16,1536]{1,0:T(8,128)} async-done(((f32[16,6144]{1,0:T(8,128)}), f32[16,1536]{1,0:T(8,128)}) %reduce-scatter.2.cloned.1.call-update) | async-done | bytes 98320 | tf_op jit(solution)/shard_map/reduce_scatter | solution.py:61
  36.1 1.0 multiply_convert_fusion
  37.0 13.6 %all_gather.12 = bf16[16,6144]{1,0:T(8,128)(2,1)S(1)} all-gather(bf16[16,1536]{1,0:T(8,128)(2,1)S(1)} %multiply_convert_fusion), channel_id=1, replica_groups=mesh['dp'=4,'kv'=4,'tp'=2] {'kv'}, dimensions={1}, use_global_device_ids=true | all-gather | bytes 245760 | tf_op jit(solution)/shard_map/all_gather | solution.py:63
  50.7 0.0 copy-start.7
  50.7 0.9 reshape.357
  51.5 0.9 fusion.80
  52.4 0.0 copy-start.9
  52.4 0.0 copy-done.11
  52.5 0.2 fusion.45
  52.6 0.1 fusion.43
  52.7 0.9 fusion.21
  53.6 0.0 copy-done.1
  53.6 0.5 fusion.32
  54.1 0.0 copy-done.7
  54.1 0.3 fusion.31
  54.5 13.2 %all-gather.2 = f32[4,12,16]{2,1,0:T(8,128)S(1)} all-gather(f32[1,12,16]{2,1,0:T(8,128)S(1)} %bitcast.105), channel_id=2, replica_groups=mesh['dp'=4,'kv'=4,'tp'=2] {'kv'}, dimensions={0}, use_global_device_ids=true | all-gather | bytes 3840 | tf_op jit(solution)/shard_map/all_gather | solution.py:91
  67.6 0.1 fusion.53
  67.7 0.0 copy-start.2
  67.7 0.9 fusion.13
  68.7 0.5 copy-done.2
  69.1 0.3 fusion.14
  69.5 14.2 %all-gather.1 = f32[4,16,12,128]{3,1,2,0:T(8,128)S(1)} all-gather(f32[1,16,12,128]{3,1,2,0:T(8,128)S(1)} %fusion.14), channel_id=3, replica_groups=mesh['dp'=4,'kv'=4,'tp'=2] {'kv'}, dimensions={0}, use_global_device_ids=true | all-gather | bytes 491520 | tf_op jit(solution)/shard_map/all_gather | solution.py:105
  83.7 1.8 %bitcast_select_fusion.1 = bf16[1,512,12,128]{3,1,2,0:T(8,128)(2,1)} fusion(bf16[1,512,12,128]{3,1,2,0:T(8,128)(2,1)S(1)} %copy-done.1, pred[512]{0:T(512)(128)(4,1)S(1)} %compare_and_fusion, bf16[1,16,1,12,128]{4,3,2,1,0:T(8,128)(2,1)S(1)} %get-tuple-element.4, s32[512]{0:T(512)S(1)} %fusion.73), kind=kOutput, calls=%fused_computation.3 | convolution fusion | flops 26746880 | bytes 3197440 | tf_op jit(solution)/shard_map/scp,sphd->schd/dot_general | solution.py:119
  85.5 0.0 copy-done.9
  85.5 0.0 copy-start.6
  85.5 1.8 %bitcast_select_fusion = bf16[1,512,12,128]{3,1,2,0:T(8,128)(2,1)} fusion(bf16[1,512,12,128]{3,1,2,0:T(8,128)(2,1)S(1)} %copy-done.2, pred[512]{0:T(512)(128)(4,1)S(1)} %compare_and_fusion, bf16[1,16,1,12,128]{4,3,2,1,0:T(8,128)(2,1)S(1)} %get-tuple-element.3, s32[512]{0:T(512)S(1)} %fusion.73), kind=kOutput, calls=%fused_computation.2 | convolution fusion | flops 26746880 | bytes 3197440 | tf_op jit(solution)/shard_map/scp,sphd->schd/dot_general | solution.py:122
  87.2 0.7 reduce.6
  87.9 1.2 %fusion.17 = f32[1,16,12,128]{3,1,2,0:T(8,128)S(1)} fusion(bf16[12,16,16]{1,2,0:T(8,128)(2,1)} %fusion.21, f32[16,12,128]{2,0,1:T(8,128)} %reduce.6, bf16[1,16,1,12,128]{4,3,2,1,0:T(8,128)(2,1)} %copy-done.9), kind=kOutput, calls=%fused_computation.18 | convolution fusion | flops 811008 | bytes 251904 | tf_op jit(solution)/shard_map/shpj,sjhd->sphd/dot_general | solution.py:107
  89.1 0.0 copy-done.6
  89.1 1.1 %convolution_convert_fusion.2 = bf16[16,512]{1,0:T(8,128)(2,1)S(1)} fusion(bf16[1536,512]{1,0:T(8,128)(2,1)S(1)} %copy-done.6, f32[2,8,12,128]{3,2,1,0:T(8,128)S(1)} %bitcast.103, bf16[16,6144]{1,0:T(8,128)(2,1)} %copy-done.7), kind=kOutput, calls=%fused_computation.25 | convolution fusion | flops 25346048 | bytes 1736704 | tf_op jit(solution)/shard_map/dot_general | solution.py:111
  90.2 4.0 %psum.15 = bf16[1,16,512]{2,1,0:T(8,128)(2,1)} all-reduce(bf16[1,16,512]{2,1,0:T(8,128)(2,1)S(1)} %bitcast.104), channel_id=1, replica_groups=mesh['dp'=4,'kv'=4,'tp'=2] {'tp'}, use_global_device_ids=true, to_apply=%region_7.8 | all-reduce | flops 8192 | bytes 32768 | tf_op jit(solution)/shard_map/psum | solution.py:113
  (7 shorter events, 0.1 us)
Async XLA Ops:
  7.2 1.4 %copy-start = (bf16[512,1536]{1,0:T(8,128)(2,1)S(1)}, bf16[512,1536]{1,0:T(8,128)(2,1)}, u32[]{:S(2)}) copy-start(bf16[512,1536]{1,0:T(8,128)(2,1)} %param.15) | copy-start | bytes 4718596
  7.2 2.5 %copy-start.8 = (bf16[1,16,512]{2,1,0:T(8,128)(2,1)S(1)}, bf16[1,16,512]{2,1,0:T(8,128)(2,1)}, u32[]{:S(2)}) copy-start(bf16[1,16,512]{2,1,0:T(8,128)(2,1)} %param.13) | copy-start | bytes 49156
  7.2 2.5 %copy-start.10 = (f32[512]{0:T(512)S(1)}, f32[512]{0:T(512)}, u32[]{:S(2)}) copy-start(f32[512]{0:T(512)} %param.14) | copy-start | bytes 6148
  7.2 2.5 %copy-start.3 = (bf16[512,1536]{1,0:T(8,128)(2,1)S(1)}, bf16[512,1536]{1,0:T(8,128)(2,1)}, u32[]{:S(2)}) copy-start(bf16[512,1536]{1,0:T(8,128)(2,1)} %param.16) | copy-start | bytes 4718596
  7.2 28.9 %reduce-scatter.2.cloned.1.call-start = ((), (), s32[]{:S(2)}) async-start(), calls=%async_computation.1 | async-start | bytes 491520 | tf_op jit(solution)/shard_map/reduce_scatter | solution.py:61
  8.6 1.6 %copy-start.4 = (bf16[512,1536]{1,0:T(8,128)(2,1)S(1)}, bf16[512,1536]{1,0:T(8,128)(2,1)}, u32[]{:S(2)}) copy-start(bf16[512,1536]{1,0:T(8,128)(2,1)} %param.17) | copy-start | bytes 4718596
  9.8 1.5 %copy-start.5 = (bf16[512,1536]{1,0:T(8,128)(2,1)S(1)}, bf16[512,1536]{1,0:T(8,128)(2,1)}, u32[]{:S(2)}) copy-start(bf16[512,1536]{1,0:T(8,128)(2,1)} %param.18) | copy-start | bytes 4718596
  11.3 1.1 %copy-start.12 = (s32[1,16]{1,0:T(1,128)S(1)}, s32[1,16]{1,0:T(1,128)}, u32[]{:S(2)}) copy-start(s32[1,16]{1,0:T(1,128)} %param.25) | copy-start | bytes 196
  11.6 40.9 %copy-start.11 = (f32[12]{0:T(128)S(1)}, f32[12]{0:T(128)}, u32[]{:S(2)}) copy-start(f32[12]{0:T(128)} %param.20) | copy-start | bytes 148
  12.4 41.2 %copy-start.1 = (bf16[1,512,12,128]{3,1,2,0:T(8,128)(2,1)S(1)}, bf16[1,512,12,128]{3,1,2,0:T(8,128)(2,1)}, u32[]{:S(2)}) copy-start(bf16[1,512,12,128]{3,1,2,0:T(8,128)(2,1)} %param.21) | copy-start | bytes 4718596
  50.7 3.5 %copy-start.7 = (bf16[16,6144]{1,0:T(8,128)(2,1)}, bf16[16,6144]{1,0:T(8,128)(2,1)S(1)}, u32[]{:S(2)}) copy-start(bf16[16,6144]{1,0:T(8,128)(2,1)S(1)} %all_gather.12) | copy-start | bytes 589828
  52.4 33.0 %copy-start.9 = (bf16[1,16,1,12,128]{4,3,2,1,0:T(8,128)(2,1)}, bf16[1,16,1,12,128]{4,3,2,1,0:T(8,128)(2,1)S(1)}, u32[]{:S(2)}) copy-start(bf16[1,16,1,12,128]{4,3,2,1,0:T(8,128)(2,1)S(1)} %get-tuple-element.3) | copy-start | bytes 147460
  67.7 1.4 %copy-start.2 = (bf16[1,512,12,128]{3,1,2,0:T(8,128)(2,1)S(1)}, bf16[1,512,12,128]{3,1,2,0:T(8,128)(2,1)}, u32[]{:S(2)}) copy-start(bf16[1,512,12,128]{3,1,2,0:T(8,128)(2,1)} %param.22) | copy-start | bytes 4718596
  85.5 3.6 %copy-start.6 = (bf16[1536,512]{1,0:T(8,128)(2,1)S(1)}, bf16[1536,512]{1,0:T(8,128)(2,1)}, u32[]{:S(2)}) copy-start(bf16[1536,512]{1,0:T(8,128)(2,1)} %param.19) | copy-start | bytes 4718596
Sparse Core Ops, SparseCore 0:
  12.5 23.5 reduce-scatter.1
